TPU v7x, 32 devices: a whole 2x2x4 slice. The times are simulated.
32 devices in a mesh: kv: 16 (over z, y, x), tp: 2 (over core).
Axes of the slice: x: 2, y: 2, z: 4, core: 2. Of those that a mesh axis runs over, the one named last changes fastest.
Arguments:
- normed: bfloat16 [8192, 4096], P('kv'), may hold values from -6 to 6
- queries: bfloat16 [8192, 1024], P('kv', 'tp'), may hold values from -6 to 6
- keys: bfloat16 [8192, 64], P('kv'), may hold values from -6 to 6
- values: bfloat16 [8192, 64], P('kv'), may hold values from -6 to 6
- attended: bfloat16 [8192, 1024], P('kv', 'tp'), may hold values from -6 to 6
- cotangent: bfloat16 [8192, 1024], P('kv', 'tp'), may hold values from -24 to 24
- log_sum: float32 [8192, 16], P('kv', 'tp'), may hold values from 6 to 8
- chosen: int32 [128, 16], P('kv'), may hold values from -1 to 127, as said below
Outputs:
- grad_queries: bfloat16 [8192, 1024], P('kv', 'tp')
- grad_keys: float32 [8192, 64], P('kv')
- grad_values: float32 [8192, 64], P('kv')
- weight_grad: float32 [4096, 1024], P('kv', 'tp')
Inputs may be any that keep to these rules, and one draw needn't show every extreme that they name: `chosen`: each row lists distinct key blocks, none after its own block, and always its own block; the listed entries come first and -1 fills the rest. A row lists from 8 to 16 blocks, fewer only where fewer blocks are open to it; on every index of kv some row lists 16 blocks where that many are open. The rows of one index of kv together list at most one block of each other index of kv's positions; every index of kv from 1 on lists a block of index 0 and a block of the index before it, and every index from half the axis on a block of the index half the axis before it.
All inputs are finite; a program needn't handle non-finite values.
Results may differ from a plain program's by a relative error of at most 0.007.
Values may be sent and summed in bfloat16 or wider, within the bound.
A program may use at most 64 MiB of HBM per device.

v0:
```python
import jax
import jax.numpy as jnp
from jax import lax
from jax.sharding import PartitionSpec as P

BLOCK = 64


def shards(normed, queries, keys, values, attended, cotangent, log_sum, chosen):
    my_rank = lax.axis_index("kv")
    peer_count = lax.axis_size("kv")
    tok_rows, model_width = normed.shape
    slot_count = chosen.shape[1]
    local_blocks = tok_rows // BLOCK
    head_dim = keys.shape[1]
    heads_here = log_sum.shape[1]
    score_scale = head_dim ** (-0.5)
    pairs_local = jnp.concatenate([keys, values], axis=1).reshape(local_blocks, BLOCK, 2 * head_dim)
    owners = chosen // local_blocks
    within = chosen % local_blocks
    listed = chosen >= 0
    remote = listed & (owners != my_rank)
    peer_ids = jnp.arange(peer_count, dtype=jnp.int32)
    matched = remote[:, :, None] & (owners[:, :, None] == peer_ids[None, None, :])
    wanted = jnp.max(jnp.where(matched, within[:, :, None] + 1, 0), axis=(0, 1))
    asked_for = (
        lax.all_to_all(
            wanted.reshape(peer_count, 1), "kv", split_axis=0, concat_axis=0, tiled=True
        )[:, 0]
        - 1
    )
    picked = jnp.maximum(asked_for, 0)
    outgoing = jnp.take(pairs_local, picked, axis=0)
    fetched = lax.all_to_all(outgoing, "kv", split_axis=0, concat_axis=0, tiled=True)
    block_table = jnp.concatenate([pairs_local, fetched], axis=0)
    slot_index = jnp.where(owners == my_rank, within, local_blocks + owners)
    slot_index = jnp.where(listed, slot_index, 0)
    gathered = jnp.take(block_table, slot_index.reshape(-1), axis=0)
    gathered = gathered.reshape(local_blocks, slot_count * BLOCK, 2 * head_dim)
    selected_keys = gathered[:, :, :head_dim]
    selected_values = gathered[:, :, head_dim:]
    query_matrix = queries.reshape(local_blocks, BLOCK, heads_here, head_dim)
    gradient_rows = cotangent.reshape(local_blocks, BLOCK, heads_here, head_dim)
    out_rows = attended.reshape(local_blocks, BLOCK, heads_here, head_dim)
    log_rows = log_sum.reshape(local_blocks, BLOCK, heads_here).transpose(0, 2, 1)
    offsets = jnp.arange(BLOCK, dtype=jnp.int32)
    query_pos = (my_rank * tok_rows + jnp.arange(tok_rows, dtype=jnp.int32)).reshape(
        local_blocks, BLOCK
    )
    key_pos = (jnp.where(listed, chosen, 0)[:, :, None] * BLOCK + offsets).reshape(
        local_blocks, slot_count * BLOCK
    )
    listed_keys = jnp.repeat(listed, BLOCK, axis=1)
    allowed = listed_keys[:, None, :] & (key_pos[:, None, :] <= query_pos[:, :, None])
    scores = (
        jnp.einsum(
            "gfvo,geo->gvfe", query_matrix, selected_keys, preferred_element_type=jnp.float32
        )
        * score_scale
    )
    probs = jnp.where(allowed[:, None], jnp.exp(scores - log_rows[:, :, :, None]), 0.0)
    reduced_probabilities = probs.astype(jnp.bfloat16)
    grad_value = jnp.einsum(
        "jpqx,jqpe->jxe", reduced_probabilities, gradient_rows, preferred_element_type=jnp.float32
    )
    probability_gradient = jnp.einsum(
        "gfvo,geo->gvfe", gradient_rows, selected_values, preferred_element_type=jnp.float32
    )
    deltas = jnp.sum(
        gradient_rows.astype(jnp.float32) * out_rows.astype(jnp.float32), axis=-1
    ).transpose(0, 2, 1)
    score_gradient = (probs * (probability_gradient - deltas[:, :, :, None]) * score_scale).astype(
        jnp.bfloat16
    )
    query_gradient = jnp.einsum(
        "xwqi,xiu->xqwu", score_gradient, selected_keys, preferred_element_type=jnp.float32
    )
    query_gradient = query_gradient.astype(jnp.bfloat16).reshape(tok_rows, heads_here * head_dim)
    key_gradient = jnp.einsum(
        "jpqx,jqpe->jxe", score_gradient, query_matrix, preferred_element_type=jnp.float32
    )
    slot_grads = jnp.concatenate([key_gradient, grad_value], axis=2).reshape(
        local_blocks * slot_count, BLOCK * 2 * head_dim
    )
    table_ids = jnp.arange(local_blocks + peer_count, dtype=jnp.int32)
    one_hot = (
        (slot_index.reshape(-1)[:, None] == table_ids[None, :]) & listed.reshape(-1)[:, None]
    ).astype(jnp.float32)
    block_sums = jnp.dot(one_hot.T, slot_grads, precision=lax.Precision.HIGHEST)
    block_sums = block_sums.reshape(local_blocks + peer_count, BLOCK, 2 * head_dim)
    own_part = block_sums[:local_blocks]
    sent_back = block_sums[local_blocks:]
    taken_by = (asked_for[:, None] == jnp.arange(local_blocks, dtype=jnp.int32)[None, :]).astype(
        jnp.float32
    )
    returned = lax.all_to_all(sent_back, "kv", split_axis=0, concat_axis=0, tiled=True)
    totals = own_part + jnp.einsum(
        "sb,skc->bkc", taken_by, returned, precision=lax.Precision.HIGHEST
    )
    totals = lax.psum(totals, "tp")
    grad_keys = totals[:, :, :head_dim].reshape(tok_rows, head_dim)
    grad_values = totals[:, :, head_dim:].reshape(tok_rows, head_dim)
    weight_grad = lax.psum_scatter(
        lax.dot_general(
            normed, query_gradient, (((0,), (0,)), ((), ())), preferred_element_type=jnp.float32
        ),
        "kv",
        scatter_dimension=0,
        tiled=True,
    )
    return (query_gradient, grad_keys, grad_values, weight_grad)


def solution(mesh):
    placed = (
        P("kv", None),
        P("kv", "tp"),
        P("kv", None),
        P("kv", None),
        P("kv", "tp"),
        P("kv", "tp"),
        P("kv", "tp"),
        P("kv", None),
    )
    return jax.shard_map(
        shards,
        mesh=mesh,
        in_specs=placed,
        out_specs=(P("kv", "tp"), P("kv", None), P("kv", None), P("kv", "tp")),
        check_vma=False,
    )
```

profile of v0, /device:TPU:0, one launch (start us, length us, event | category | flops | bytes accessed | tf_op | source)
XLA Modules:
  0.0 311.9 jit_solution(15247544557536158167)
XLA Ops:
  8.0 0.7 select_multiply_fusion
  8.7 1.3 compare_and_fusion.2
  10.0 0.1 select_reduce_fusion
  10.1 0.7 copy.67
  10.8 8.3 %all-to-all-start = ((s32[16,1,1]{2,1,0:T(1,128)}), s32[16,1,1]{2,1,0:T(1,128)S(1)}, u32[]{:S(2)}, u32[]{:S(2)}) async-start(s32[16,1,1]{2,1,0:T(1,128)} %copy.67), calls=%async_computation | async-start | bytes 16384 | tf_op jit(solution)/shard_map/all_to_all | solution.py:27
  19.1 1.0 copy.66
  20.1 1.0 copy.65
  21.1 0.1 reshape.147
  21.2 0.6 pad_clamp_fusion
  21.8 1.6 reshape.150
  23.4 1.5 reshape.156
  25.0 0.1 pad_maximum_fusion.2
  25.1 0.6 multiply_reduce_fusion
  25.7 0.6 all-to-all-done
  26.4 0.7 add_reduce_fusion
  27.1 0.6 gather_fusion
  27.7 0.8 broadcast_select_fusion.1
  28.5 6.3 %all-to-all-start.1 = ((bf16[16,64,128]{2,1,0:T(8,128)(2,1)}), bf16[16,64,128]{2,1,0:T(8,128)(2,1)S(1)}, u32[]{:S(2)}, u32[]{:S(2)}) async-start(bf16[16,64,128]{2,1,0:T(8,128)(2,1)} %broadcast_select_fusion.1), calls=%async_computation.1 | async-start | bytes 524288 | tf_op jit(solution)/shard_map/all_to_all | solution.py:34
  34.8 1.5 copy.75
  36.3 0.1 reshape.152
  36.3 0.7 and.68
  37.1 1.6 reshape.148
  38.7 0.8 copy.74
  39.5 0.1 broadcast_in_dim.66
  39.6 0.1 broadcast_in_dim.67
  39.7 0.1 copy.72
  39.8 0.1 reshape.149
  39.9 0.1 add.106
  40.0 0.1 add.107
  40.2 0.1 broadcast_in_dim.74
  40.2 0.1 and.65
  40.4 1.3 compare_and_fusion
  41.6 2.4 all-to-all-done.1
  44.1 2.3 gather_fusion.1
  46.4 3.9 %copy.68 = bf16[8,1024,128]{1,2,0:T(8,128)(2,1)} copy(bf16[8,1024,128]{2,1,0:T(8,128)(2,1)} %bitcast.78) | data formatting | bytes 4194304 | tf_op jit(solution)/shard_map/jit(_take)/gather | solution.py:38
  50.3 1.8 broadcast_select_fusion
  52.1 2.4 fusion.13
  54.5 5.7 %copy-done.1 = f32[8,1024,64,8]{1,2,3,0:T(8,128)} copy-done((f32[8,1024,64,8]{1,2,3,0:T(8,128)}, f32[8,1024,64,8]{1,2,3,0:T(8,128)S(1)}, u32[]{:S(2)}) %copy-start.1) | copy-done | bytes 16777240
  60.2 4.8 %fusion.9 = f32[8,1024,64]{1,2,0:T(8,128)} fusion(bf16[8,64,8,64]{1,3,2,0:T(8,128)(2,1)S(1)} %copy-done.7, f32[8,1024,64,8]{1,2,3,0:T(8,128)S(1)} %fusion.13, f32[8,8,64]{2,1,0:T(8,128)S(1)} %bitcast.82, pred[8,64,1024]{2,1,0:T(8,128)(4,1)S(1)} %copy-done.8), kind=kOutput, calls=%fused_computation.17 | convolution fusion | flops 553648128 | bytes 19939328 | tf_op jit(solution)/shard_map/jpqx,jqpe->jxe/dot_general | solution.py:63
  65.0 10.3 %fusion.2 = bf16[8,8,64,1024]{3,2,1,0:T(8,128)(2,1)S(1)} fusion(f32[8,1024,64,8]{1,2,3,0:T(8,128)} %copy-done.1, bf16[8,64,8,64]{1,3,2,0:T(8,128)(2,1)S(1)} %copy-done.7, f32[8,8,64]{2,1,0:T(8,128)S(1)} %copy.72, f32[8,8,64]{2,1,0:T(8,128)S(1)} %bitcast.83, pred[8,64,1024]{2,1,0:T(8,128)(4,1)S(1)} %copy-done.8, bf16[8,1024,128]{1,2,0:T(8,128)(2,1)} %copy-done.2), kind=kOutput, calls=%fused_computation.5 | convolution fusion | flops 566231040 | bytes 27295744 | tf_op jit(solution)/shard_map/gfvo,geo->gvfe/dot_general | solution.py:66
  75.3 1.6 convolution_bitcast_fusion.1
  76.9 1.9 copy-done
  78.8 2.5 pad_maximum_fusion
  81.3 5.3 %copy.76 = f32[8,1024,128]{2,1,0:T(8,128)} copy(f32[8,1024,128]{1,2,0:T(8,128)} %pad_maximum_fusion) | data formatting | bytes 8388608 | tf_op jit(solution)/shard_map/concatenate | solution.py:82
  86.6 4.9 %reshape.153 = f32[128,8192]{1,0:T(8,128)} reshape(f32[8,1024,128]{2,1,0:T(8,128)} %copy.76) | data formatting | bytes 8388608 | tf_op jit(solution)/shard_map/reshape | solution.py:82
  91.6 3.8 %fusion.17 = f32[24,8192]{1,0:T(8,128)S(1)} fusion(f32[128,8192]{1,0:T(8,128)} %reshape.153, s32[128]{0:T(128)S(1)} %reshape.152, pred[128]{0:T(512)(128)(4,1)S(1)} %and.68), kind=kOutput, calls=%fused_computation.36 | convolution fusion | flops 301996032 | bytes 4981376 | tf_op jit(solution)/shard_map/dot_general | solution.py:89
  95.4 1.0 copy-done.4
  96.4 0.9 copy.85
  97.3 4.5 %all-to-all-start.2 = ((f32[16,64,128]{2,1,0:T(8,128)}), f32[16,64,128]{2,1,0:T(8,128)}, u32[]{:S(2)}, u32[]{:S(2)}) async-start(f32[16,64,128]{2,1,0:T(8,128)} %bitcast.25), calls=%async_computation.2 | async-start | bytes 1048576 | tf_op jit(solution)/shard_map/all_to_all | solution.py:96
  101.8 0.3 all-reduce.2.cloned.1.call-start
  102.1 7.5 %fusion.12 = bf16[8,64,8,64]{1,3,2,0:T(8,128)(2,1)S(1)} fusion(bf16[8,8,64,1024]{3,2,1,0:T(8,128)(2,1)} %copy-done, bf16[8,1024,128]{1,2,0:T(8,128)(2,1)S(1)} %copy-done.3), kind=kOutput, calls=%fused_computation.20 | convolution fusion | flops 537133056 | bytes 9961472 | tf_op jit(solution)/shard_map/xwqi,xiu->xqwu/dot_general | solution.py:75
  109.6 0.7 copy.73
  110.4 0.6 reshape.151
  111.0 5.0 %all-to-all-done.2 = f32[16,64,128]{2,1,0:T(8,128)} async-done(((f32[16,64,128]{2,1,0:T(8,128)}), f32[16,64,128]{2,1,0:T(8,128)}, u32[]{:S(2)}, u32[]{:S(2)}) %all-to-all-start.2) | async-done | bytes 524320 | tf_op jit(solution)/shard_map/all_to_all | solution.py:96
  115.9 2.4 convolution_add_fusion
  118.4 7.8 %convolution_bitcast_fusion = f32[4096,512]{0,1:T(8,128)} fusion(bf16[512,512]{1,0:T(8,128)(2,1)S(1)} %reshape.151, bf16[512,4096]{1,0:T(8,128)(2,1)} %param.8), kind=kOutput, calls=%fused_computation.12 | convolution fusion | flops 2147483648 | bytes 13107200 | tf_op jit(solution)/shard_map/dot_general | solution.py:104
  126.2 8.7 %all-reduce.2.cloned.1.call-done = f32[8,64,128]{2,0,1:T(8,128)} async-done(((f32[8,64,128]{2,0,1:T(8,128)}), f32[8,64,128]{2,0,1:T(8,128)}) %all-reduce.2.cloned.1.call-update) | async-done | bytes 262160 | tf_op jit(solution)/shard_map/psum | solution.py:100
  135.0 1.2 fusion.29
  136.1 0.2 copy.78
  136.3 0.8 reshape.154
  137.1 0.2 copy.79
  137.3 0.8 reshape.155
  138.0 164.4 %reduce-scatter.2.cloned.1.call-done = f32[256,512]{0,1:T(8,128)} async-done(((f32[4096,512]{0,1:T(8,128)}), f32[256,512]{0,1:T(8,128)}) %reduce-scatter.2.cloned.1.call-update) | async-done | bytes 524304 | tf_op jit(solution)/shard_map/reduce_scatter | solution.py:103
  302.4 2.0 copy.80
  (41 shorter events, 0.3 us)
Async XLA Ops:
  8.7 2.1 copy-start.10
  10.8 15.6 %all-to-all-start = ((s32[16,1,1]{2,1,0:T(1,128)}), s32[16,1,1]{2,1,0:T(1,128)S(1)}, u32[]{:S(2)}, u32[]{:S(2)}) async-start(s32[16,1,1]{2,1,0:T(1,128)} %copy.67), calls=%async_computation | async-start | bytes 16384 | tf_op jit(solution)/shard_map/all_to_all | solution.py:27
  25.7 13.8 %copy-start.12 = (pred[8,16]{1,0:T(8,128)(4,1)S(1)}, pred[8,16]{1,0:T(8,128)(4,1)}, u32[]{:S(2)}) copy-start(pred[8,16]{1,0:T(8,128)(4,1)} %get-tuple-element.28) | copy-start | bytes 388
  25.7 14.1 %copy-start.9 = (f32[512,8]{0,1:T(8,128)S(1)}, f32[512,8]{0,1:T(8,128)}, u32[]{:S(2)}) copy-start(f32[512,8]{0,1:T(8,128)} %param.14) | copy-start | bytes 49156
  25.7 14.4 %copy-start.11 = (pred[8,16]{1,0:T(8,128)(4,1)S(1)}, pred[8,16]{1,0:T(8,128)(4,1)}, u32[]{:S(2)}) copy-start(pred[8,16]{1,0:T(8,128)(4,1)} %copy-done.10) | copy-start | bytes 388
  27.0 12.8 %copy-start.13 = (s32[16]{0:T(128)}, s32[16]{0:T(128)S(1)}, u32[]{:S(2)}) copy-start(s32[16]{0:T(128)S(1)} %get-tuple-element.24) | copy-start | bytes 196
  28.5 15.6 %all-to-all-start.1 = ((bf16[16,64,128]{2,1,0:T(8,128)(2,1)}), bf16[16,64,128]{2,1,0:T(8,128)(2,1)S(1)}, u32[]{:S(2)}, u32[]{:S(2)}) async-start(bf16[16,64,128]{2,1,0:T(8,128)(2,1)} %broadcast_select_fusion.1), calls=%async_computation.1 | async-start | bytes 524288 | tf_op jit(solution)/shard_map/all_to_all | solution.py:34
  52.1 2.4 copy-start.2
  52.1 8.1 %copy-start.7 = (bf16[8,64,8,64]{1,3,2,0:T(8,128)(2,1)S(1)}, bf16[8,64,8,64]{1,3,2,0:T(8,128)(2,1)}, u32[]{:S(2)}) copy-start(bf16[8,64,8,64]{1,3,2,0:T(8,128)(2,1)} %copy.75) | copy-start | bytes 1572868
  52.1 8.1 %copy-start.8 = (pred[8,64,1024]{2,1,0:T(8,128)(4,1)S(1)}, pred[8,64,1024]{2,1,0:T(8,128)(4,1)}, u32[]{:S(2)}) copy-start(pred[8,64,1024]{2,1,0:T(8,128)(4,1)} %compare_and_fusion) | copy-start | bytes 1572868
  54.5 5.7 %copy-start.1 = (f32[8,1024,64,8]{1,2,3,0:T(8,128)}, f32[8,1024,64,8]{1,2,3,0:T(8,128)S(1)}, u32[]{:S(2)}) copy-start(f32[8,1024,64,8]{1,2,3,0:T(8,128)S(1)} %fusion.13) | copy-start | bytes 50331652
  75.3 3.5 %copy-start = (bf16[8,8,64,1024]{3,2,1,0:T(8,128)(2,1)}, bf16[8,8,64,1024]{3,2,1,0:T(8,128)(2,1)S(1)}, u32[]{:S(2)}) copy-start(bf16[8,8,64,1024]{3,2,1,0:T(8,128)(2,1)S(1)} %fusion.2) | copy-start | bytes 25165828
  75.3 3.5 %copy-start.6 = (f32[8,1024,64]{1,2,0:T(8,128)S(1)}, f32[8,1024,64]{1,2,0:T(8,128)}, u32[]{:S(2)}) copy-start(f32[8,1024,64]{1,2,0:T(8,128)} %fusion.9) | copy-start | bytes 6291460
  91.6 10.5 %copy-start.3 = (bf16[8,1024,128]{1,2,0:T(8,128)(2,1)S(1)}, bf16[8,1024,128]{1,2,0:T(8,128)(2,1)}, u32[]{:S(2)}) copy-start(bf16[8,1024,128]{1,2,0:T(8,128)(2,1)} %copy-done.2) | copy-start | bytes 6291460
  95.4 1.0 copy-start.4
  97.3 18.6 %all-to-all-start.2 = ((f32[16,64,128]{2,1,0:T(8,128)}), f32[16,64,128]{2,1,0:T(8,128)}, u32[]{:S(2)}, u32[]{:S(2)}) async-start(f32[16,64,128]{2,1,0:T(8,128)} %bitcast.25), calls=%async_computation.2 | async-start | bytes 1048576 | tf_op jit(solution)/shard_map/all_to_all | solution.py:96
  101.8 14.1 %copy-start.14 = (s32[16]{0:T(128)S(1)}, s32[16]{0:T(128)}, u32[]{:S(2)}) copy-start(s32[16]{0:T(128)} %copy-done.13) | copy-start | bytes 196
  101.8 33.1 %all-reduce.2.cloned.1.call-start = ((), (), s32[]{:S(2)}) async-start(), calls=%async_computation.4 | async-start | bytes 524288 | tf_op jit(solution)/shard_map/psum | solution.py:100
  111.0 15.2 %copy-start.5 = (bf16[512,512]{1,0:T(8,128)(2,1)}, bf16[512,512]{1,0:T(8,128)(2,1)S(1)}, u32[]{:S(2)}) copy-start(bf16[512,512]{1,0:T(8,128)(2,1)S(1)} %reshape.151) | copy-start | bytes 1572868
  118.4 184.0 %reduce-scatter.2.cloned.1.call-start = ((), (), s32[]{:S(2)}) async-start(), calls=%async_computation.5 | async-start | bytes 8912896 | tf_op jit(solution)/shard_map/reduce_scatter | solution.py:103
Sparse Core Ops, SparseCore 0:
  118.5 16.4 all-reduce.1
Sparse Core Ops, SparseCore 1:
  126.3 176.0 reduce-scatter.1
where the time goes:
time: 314 us; the launch traced here: 312 us
  waiting for transfers between devices  181 us (58%)
  local copies, waits for them, and re-layouts  44.4 us (14%)
  matrix products  40.5 us (13%)
  starting transfers between devices  19.4 us (6%)
  between operations  15.8 us (5%)
  other arithmetic  10.5 us (3%)
    reduce_scatter x1, waiting for transfers between devices, shards(): lax.psum_scatter(lax.dot_general(normed, query_gradient, (((0,), (0,)), (...  164 us
    unnamed x35, local copies, waits for them, and re-layouts  13.5 us
    dot_general x1, matrix products, shards(): jnp.einsum('gfvo,geo->gvfe', gradient_rows, selected_values, preferred_el...  10.3 us
    psum x1, waiting for transfers between devices, shards(): totals = lax.psum(totals, 'tp')  8.74 us
    all_to_all x1, starting transfers between devices, shards(): lax.all_to_all(wanted.reshape(peer_count, 1), 'kv', split_axis=0, concat_...  8.34 us
    dot_general x1, matrix products, shards(): lax.dot_general(normed, query_gradient, (((0,), (0,)), ((), ())), preferr...  7.79 us
    dot_general x1, matrix products, shards(): jnp.einsum('xwqi,xiu->xqwu', score_gradient, selected_keys, preferred_ele...  7.48 us
    all_to_all x1, starting transfers between devices, shards(): lax.all_to_all(outgoing, 'kv', split_axis=0, concat_axis=0, tiled=True)  6.29 us
  transfers between devices with their start and end apart: 5, of which 5 were waited for; matrix products, arithmetic and copies ran while one was open for 11% of the time, Pallas kernels for 0%

commit v1 on v0

v1 whole, which is shorter than its diff:
```python
import functools

import jax
import jax.numpy as jnp
from jax import lax
from jax.experimental import pallas as pl
from jax.experimental.pallas import tpu as pltpu
from jax.sharding import PartitionSpec as P

BLOCK = 64
GROUP = 4
NT = (((1,), (1,)), ((), ()))
TN = (((0,), (0,)), ((), ()))


def greet(n, peers_tp):
    me = lax.axis_index("kv")
    barrier = pltpu.get_barrier_semaphore()

    def hello(k, _):
        pl.semaphore_signal(barrier, inc=1, device_id={"kv": lax.rem(me + k, n)})
        return 0

    lax.fori_loop(1, n, hello, 0)
    if peers_tp > 1:
        mine = lax.axis_index("tp")
        for k in range(1, peers_tp):
            pl.semaphore_signal(
                barrier, inc=1, device_id={"tp": lax.rem(mine + k, peers_tp)}
            )
    return barrier


def fetch_kernel(n, nb, keys_ref, values_ref, want_ref, table_ref, asked_ref, out_buf, s1, r1, s2, r2):
    me = lax.axis_index("kv")
    barrier = greet(n, 1)
    pairs = jnp.concatenate([keys_ref[...], values_ref[...]], axis=1)
    for b in range(nb):
        table_ref[b] = pairs[b * BLOCK : (b + 1) * BLOCK]

    def blank(p, _):
        table_ref[nb + p] = jnp.zeros(table_ref.shape[1:], table_ref.dtype)
        return 0

    lax.fori_loop(me, n, blank, 0)

    def unasked(p, _):
        asked_ref[p] = jnp.full(asked_ref.shape[1:], -1, jnp.int32)
        return 0

    lax.fori_loop(0, me + 1, unasked, 0)
    pl.semaphore_wait(barrier, n - 1)

    def request(p):
        return pltpu.make_async_remote_copy(
            src_ref=want_ref.at[p],
            dst_ref=asked_ref.at[me],
            send_sem=s1.at[p],
            recv_sem=r1.at[me],
            device_id={"kv": p},
        )

    def asked_from(q):
        return pltpu.make_async_remote_copy(
            src_ref=want_ref.at[q],
            dst_ref=asked_ref.at[q],
            send_sem=s1.at[q],
            recv_sem=r1.at[q],
            device_id={"kv": q},
        )

    def reply(q):
        return pltpu.make_async_remote_copy(
            src_ref=out_buf.at[q],
            dst_ref=table_ref.at[nb + me],
            send_sem=s2.at[q],
            recv_sem=r2.at[me],
            device_id={"kv": q},
        )

    def reply_from(p):
        return pltpu.make_async_remote_copy(
            src_ref=out_buf.at[p],
            dst_ref=table_ref.at[nb + p],
            send_sem=s2.at[p],
            recv_sem=r2.at[p],
            device_id={"kv": p},
        )

    def step(fn):
        def body(i, _):
            fn(i)
            return 0

        return body

    lax.fori_loop(0, me, step(lambda p: request(p).start()), 0)

    def answer(q):
        asked_from(q).wait_recv()
        tile = asked_ref[q]
        wide = jnp.concatenate([tile] * (BLOCK // tile.shape[0]), axis=0)
        picked = jnp.zeros(wide.shape, jnp.float32)
        for b in range(nb):
            picked = jnp.where(wide == b, table_ref[b].astype(jnp.float32), picked)
        out_buf[q] = picked.astype(out_buf.dtype)
        reply(q).start()

    lax.fori_loop(me + 1, n, step(answer), 0)
    lax.fori_loop(0, me, step(lambda p: request(p).wait_send()), 0)
    lax.fori_loop(me + 1, n, step(lambda q: reply(q).wait_send()), 0)
    lax.fori_loop(0, me, step(lambda p: reply_from(p).wait_recv()), 0)


def attention_kernel(
    heads, nb, n, slots, limits, counts,
    q_ref, o_ref, g_ref, l_ref, table_ref, gq_ref, own_ref, back_ref, acc, dqt,
):
    g = pl.program_id(0)
    rows = heads * BLOCK
    scale = BLOCK ** (-0.5)

    @pl.when(g == 0)
    def _():
        acc[...] = jnp.zeros_like(acc)

    def stack(ref):
        full = ref[...]
        return jnp.concatenate([full[:, h * BLOCK : (h + 1) * BLOCK] for h in range(heads)], axis=0)

    q = stack(q_ref)
    go = stack(g_ref)
    prod = go.astype(jnp.float32) * stack(o_ref).astype(jnp.float32)
    high = prod.astype(jnp.bfloat16)
    low = (prod - high.astype(jnp.float32)).astype(jnp.bfloat16)
    ones = jnp.ones((8, BLOCK), jnp.bfloat16)
    delta = (
        lax.dot_general(ones, high, NT, preferred_element_type=jnp.float32)
        + lax.dot_general(ones, low, NT, preferred_element_type=jnp.float32)
    )[0:1]
    logs = l_ref[0]
    ahead = (
        lax.broadcasted_iota(jnp.int32, (BLOCK, rows), 1) % BLOCK
        - lax.broadcasted_iota(jnp.int32, (BLOCK, rows), 0)
    )
    dqt[...] = jnp.zeros_like(dqt)
    for c in range(slots.shape[1] // GROUP):

        @pl.when(counts[g] > c * GROUP)
        def _():
            ids = [slots[g, c * GROUP + i] for i in range(GROUP)]
            pairs = jnp.concatenate([table_ref[s] for s in ids], axis=0)
            k = pairs[:, :BLOCK]
            v = pairs[:, BLOCK:]
            s = lax.dot_general(k, q, NT, preferred_element_type=jnp.float32)
            dp = lax.dot_general(v, go, NT, preferred_element_type=jnp.float32)
            e = jnp.exp(s * scale - logs)
            p = jnp.concatenate(
                [
                    jnp.where(
                        ahead >= limits[g, c * GROUP + i], e[i * BLOCK : (i + 1) * BLOCK], 0.0
                    )
                    for i in range(GROUP)
                ],
                axis=0,
            )
            ds = (p * (dp - delta) * scale).astype(jnp.bfloat16)
            dk = jnp.dot(ds, q, preferred_element_type=jnp.float32)
            dv = jnp.dot(p.astype(jnp.bfloat16), go, preferred_element_type=jnp.float32)
            dqt[...] += lax.dot_general(k, ds, TN, preferred_element_type=jnp.float32)
            dkv = jnp.concatenate([dk, dv], axis=1)
            for i in range(GROUP):
                acc[ids[i]] += dkv[i * BLOCK : (i + 1) * BLOCK]

    dq = dqt[...].T.astype(jnp.bfloat16)
    gq_ref[...] = jnp.concatenate([dq[h * BLOCK : (h + 1) * BLOCK] for h in range(heads)], axis=1)

    @pl.when(g == nb - 1)
    def _():
        own_ref[...] = acc[:nb]
        back_ref[...] = acc[nb:].astype(back_ref.dtype)


def reduce_kernel(
    n, tp, nb, normed_ref, gq_ref, own_ref, back_ref, asked_ref,
    wg_ref, dk_ref, dv_ref,
    gqt, send1, recv1, own, send2, recv2, send3, recv3, came, total, others,
    ss1, rs1, ss2, rs2, ss3, rs3, ssb, rsb, sst, rst,
):
    me = lax.axis_index("kv")
    mine = lax.axis_index("tp")
    zs = n // 4
    x = lax.rem(me, 2)
    y = lax.rem(me // 2, 2)
    z = me // 4
    barrier = greet(n, tp)
    half = gqt.shape[1]
    width = send1.shape[3]
    turned = gq_ref[...].T
    gqt[0] = turned[:half]
    gqt[1] = turned[half:]

    def index(zz, a, b, h):
        return zz * 4 + (b * 2 + a if h == 0 else a * 2 + b)

    coords = ((x, y), (y, x))

    def chunk_at(h, i, a):
        b = coords[h][1]
        bb = jnp.where(i < zs, 1 - b, b)
        zz = lax.rem(z + 1 + lax.rem(i, zs), zs)
        return index(zz, a, bb, h)

    def part(h, chunk):
        cols = pl.ds(pl.multiple_of(chunk * width, 128), width)
        return jnp.dot(gqt[h], normed_ref[:, cols], preferred_element_type=jnp.float32)

    def copy1(h, i):
        a, b = coords[h]
        return pltpu.make_async_remote_copy(
            src_ref=send1.at[h, i], dst_ref=recv1.at[h, i],
            send_sem=ss1.at[h, i], recv_sem=rs1.at[h, i],
            device_id={"kv": index(z, 1 - a, b, h)},
        )

    def copy2(h, i):
        a, b = coords[h]
        return pltpu.make_async_remote_copy(
            src_ref=send2.at[h, i], dst_ref=recv2.at[h, i],
            send_sem=ss2.at[h, i], recv_sem=rs2.at[h, i],
            device_id={"kv": index(z, a, 1 - b, h)},
        )

    def copy3(h, i):
        a, b = coords[h]
        return pltpu.make_async_remote_copy(
            src_ref=send3.at[h, i], dst_ref=recv3.at[h, i],
            send_sem=ss3.at[h, i], recv_sem=rs3.at[h, i],
            device_id={"kv": index(lax.rem(z + 1 + i, zs), a, b, h)},
        )

    def back_to(p):
        return pltpu.make_async_remote_copy(
            src_ref=back_ref.at[p], dst_ref=came.at[me],
            send_sem=ssb.at[p], recv_sem=rsb.at[me], device_id={"kv": p},
        )

    def back_from(q):
        return pltpu.make_async_remote_copy(
            src_ref=back_ref.at[q], dst_ref=came.at[q],
            send_sem=ssb.at[q], recv_sem=rsb.at[q], device_id={"kv": q},
        )

    def across(k):
        return pltpu.make_async_remote_copy(
            src_ref=total, dst_ref=others.at[k - 1],
            send_sem=sst.at[k - 1], recv_sem=rst.at[k - 1],
            device_id={"tp": lax.rem(mine + k, tp)},
        )

    def loop(start, stop, fn):
        def body(i, _):
            fn(i)
            return 0

        lax.fori_loop(start, stop, body, 0)

    def prepare(i):
        for h in range(2):
            send1[h, i] = part(h, chunk_at(h, i, 1 - coords[h][0])).astype(send1.dtype)

    prepare(0)
    pl.semaphore_wait(barrier, n - 1 + tp - 1)
    for h in range(2):
        copy1(h, 0).start()

    def first(i):
        prepare(i)
        for h in range(2):
            copy1(h, i).start()

    loop(1, 2 * zs, first)
    loop(0, me, lambda p: back_to(p).start())

    def keep(i):
        for h in range(2):
            own[h, i] = part(h, chunk_at(h, i, coords[h][0]))

    loop(0, 2 * zs, keep)

    def second(i):
        for h in range(2):
            copy1(h, i).wait_recv()
            send2[h, i] = (own[h, i] + recv1[h, i].astype(jnp.float32)).astype(send2.dtype)
            copy2(h, i).start()

    loop(0, zs, second)

    total[...] = own_ref[...]

    def gather(q):
        back_from(q).wait_recv()
        tile = asked_ref[q]
        wide = jnp.concatenate([tile] * (BLOCK // tile.shape[0]), axis=0)
        block = came[q].astype(jnp.float32)
        for b in range(nb):
            total[b] += jnp.where(wide == b, block, 0.0)

    loop(me + 1, n, gather)
    for k in range(1, tp):
        across(k).start()

    def joined(h, i):
        copy1(h, zs + i).wait_recv()
        copy2(h, i).wait_recv()
        return (
            own[h, zs + i]
            + recv1[h, zs + i].astype(jnp.float32)
            + recv2[h, i].astype(jnp.float32)
        )

    def third(i):
        for h in range(2):
            send3[h, i] = joined(h, i).astype(send3.dtype)
            copy3(h, i).start()

    loop(0, zs - 1, third)

    for k in range(1, tp):
        across(k).wait_recv()
    summed = total[...]
    for k in range(1, tp):
        summed = summed + others[k - 1]
    flat = summed.reshape(nb * BLOCK, 2 * BLOCK)
    dk_ref[...] = flat[:, :BLOCK]
    dv_ref[...] = flat[:, BLOCK:]

    for h in range(2):
        own[h, 0] = joined(h, zs - 1)

    def fourth(i):
        for h in range(2):
            copy3(h, i).wait_recv()
            own[h, 0] += recv3[h, i].astype(jnp.float32)

    loop(0, zs - 1, fourth)
    whole = jnp.concatenate([own[0, 0], own[1, 0]], axis=0)
    wg_ref[...] = whole.T

    for h in range(2):
        loop(0, 2 * zs, lambda i: copy1(h, i).wait_send())
        loop(0, zs, lambda i: copy2(h, i).wait_send())
        loop(0, zs - 1, lambda i: copy3(h, i).wait_send())
    loop(0, me, lambda p: back_to(p).wait_send())
    for k in range(1, tp):
        across(k).wait_send()


def shards(n, tp, normed, queries, keys, values, attended, cotangent, log_sum, chosen):
    me = lax.axis_index("kv")
    tok_rows, model_width = normed.shape
    slot_count = chosen.shape[1]
    nb = tok_rows // BLOCK
    heads = log_sum.shape[1]
    cols = queries.shape[1]
    pair = 2 * BLOCK
    vmem = pl.BlockSpec(memory_space=pltpu.VMEM)
    dma = pltpu.SemaphoreType.DMA

    owners = chosen // nb
    within = chosen % nb
    listed = chosen >= 0
    remote = listed & (owners != me)
    peer_ids = jnp.arange(n, dtype=jnp.int32)
    matched = remote[:, :, None] & (owners[:, :, None] == peer_ids)
    wanted = jnp.max(jnp.where(matched, within[:, :, None], -1), axis=(0, 1))
    wanted = jnp.broadcast_to(wanted[:, None, None], (n, 8, 128))
    slots = jnp.where(listed, jnp.where(owners == me, within, nb + owners), 0)
    row_base = (me * nb + jnp.arange(nb, dtype=jnp.int32))[:, None]
    limits = jnp.where(listed, (chosen - row_base) * BLOCK, 4 * BLOCK)
    counts = jnp.sum(listed.astype(jnp.int32), axis=1)

    table, asked = pl.pallas_call(
        functools.partial(fetch_kernel, n, nb),
        out_shape=(
            jax.ShapeDtypeStruct((nb + n, BLOCK, pair), jnp.bfloat16),
            jax.ShapeDtypeStruct((n, 8, 128), jnp.int32),
        ),
        in_specs=[vmem] * 3,
        out_specs=(vmem, vmem),
        scratch_shapes=[pltpu.VMEM((n, BLOCK, pair), jnp.bfloat16)] + [dma((n,))] * 4,
        compiler_params=pltpu.CompilerParams(collective_id=0, has_side_effects=True),
        name="fetch",
    )(keys, values, wanted)

    logs = log_sum.reshape(nb, BLOCK, heads).transpose(0, 2, 1).reshape(nb, 1, heads * BLOCK)
    rows_spec = pl.BlockSpec((BLOCK, cols), lambda g, *_: (g, 0))
    gq, own_part, back = pl.pallas_call(
        functools.partial(attention_kernel, heads, nb, n),
        out_shape=(
            jax.ShapeDtypeStruct((tok_rows, cols), jnp.bfloat16),
            jax.ShapeDtypeStruct((nb, BLOCK, pair), jnp.float32),
            jax.ShapeDtypeStruct((n, BLOCK, pair), jnp.bfloat16),
        ),
        grid_spec=pltpu.PrefetchScalarGridSpec(
            num_scalar_prefetch=3,
            grid=(nb,),
            in_specs=[
                rows_spec,
                rows_spec,
                rows_spec,
                pl.BlockSpec((1, 1, heads * BLOCK), lambda g, *_: (g, 0, 0)),
                pl.BlockSpec((nb + n, BLOCK, pair), lambda g, *_: (0, 0, 0)),
            ],
            out_specs=(
                rows_spec,
                pl.BlockSpec((nb, BLOCK, pair), lambda g, *_: (0, 0, 0)),
                pl.BlockSpec((n, BLOCK, pair), lambda g, *_: (0, 0, 0)),
            ),
            scratch_shapes=[
                pltpu.VMEM((nb + n, BLOCK, pair), jnp.float32),
                pltpu.VMEM((BLOCK, heads * BLOCK), jnp.float32),
            ],
        ),
        compiler_params=pltpu.CompilerParams(dimension_semantics=("arbitrary",)),
        name="attention",
    )(slots, limits, counts, queries, attended, cotangent, logs, table)

    zs = n // 4
    half = cols // 2
    width = model_width // n
    low = jnp.bfloat16
    wide = jnp.float32
    weight_grad, grad_keys, grad_values = pl.pallas_call(
        functools.partial(reduce_kernel, n, tp, nb),
        out_shape=(
            jax.ShapeDtypeStruct((width, cols), wide),
            jax.ShapeDtypeStruct((tok_rows, BLOCK), wide),
            jax.ShapeDtypeStruct((tok_rows, BLOCK), wide),
        ),
        in_specs=[vmem] * 5,
        out_specs=(vmem, vmem, vmem),
        scratch_shapes=[
            pltpu.VMEM((2, half, tok_rows), low),
            pltpu.VMEM((2, 2 * zs, half, width), low),
            pltpu.VMEM((2, 2 * zs, half, width), low),
            pltpu.VMEM((2, 2 * zs, half, width), wide),
            pltpu.VMEM((2, zs, half, width), low),
            pltpu.VMEM((2, zs, half, width), low),
            pltpu.VMEM((2, zs - 1, half, width), low),
            pltpu.VMEM((2, zs - 1, half, width), low),
            pltpu.VMEM((n, BLOCK, pair), low),
            pltpu.VMEM((nb, BLOCK, pair), wide),
            pltpu.VMEM((tp - 1, nb, BLOCK, pair), wide),
            dma((2, 2 * zs)), dma((2, 2 * zs)),
            dma((2, zs)), dma((2, zs)),
            dma((2, zs - 1)), dma((2, zs - 1)),
            dma((n,)), dma((n,)),
            dma((tp - 1,)), dma((tp - 1,)),
        ],
        compiler_params=pltpu.CompilerParams(
            collective_id=1, has_side_effects=True, vmem_limit_bytes=56 * 1024 * 1024
        ),
        name="reduce",
    )(normed, gq, own_part, back, asked)
    return (gq, grad_keys, grad_values, weight_grad)


def solution(mesh):
    placed = (
        P("kv", None),
        P("kv", "tp"),
        P("kv", None),
        P("kv", None),
        P("kv", "tp"),
        P("kv", "tp"),
        P("kv", "tp"),
        P("kv", None),
    )
    return jax.shard_map(
        functools.partial(shards, mesh.shape["kv"], mesh.shape["tp"]),
        mesh=mesh,
        in_specs=placed,
        out_specs=(P("kv", "tp"), P("kv", None), P("kv", None), P("kv", "tp")),
        check_vma=False,
    )
```

time: 314 us -> 112 us (0.36)
  waiting for transfers between devices: 181 us -> 0 us
  Pallas kernels: 0 us -> 95.8 us
  matrix products: 40.5 us -> 0 us
  local copies, waits for them, and re-layouts: 44.4 us -> 10.7 us
  starting transfers between devices: 19.4 us -> 0 us
  between operations: 15.8 us -> 0.67 us
  other arithmetic: 10.5 us -> 2.81 us
    reduce_scatter x1 -> x0, waiting for transfers between devices: 164 us -> none  [shards(): lax.psum_scatter(lax.dot_general(normed, query_gradient, (((0,), (0,)), (...]
    pallas_call x0 -> x3, Pallas kernels: none -> 95.8 us  [the longest x1 66 us: shards(): pl.pallas_call(functools.partial(reduce_kernel, n, tp, nb), out_shape=(ja...]
    dot_general x8 -> x0, matrix products: 40.5 us -> none  [the longest x1 10.3 us: shards(): jnp.einsum('gfvo,geo->gvfe', gradient_rows, selected_values, preferred_el...]
    all_to_all x3 -> x0, starting transfers between devices: 19.1 us -> none  [the longest x1 8.34 us: shards(): lax.all_to_all(wanted.reshape(peer_count, 1), 'kv', split_axis=0, concat_...]
    reshape x12 -> x3, local copies, waits for them, and re-layouts: 12.9 us -> 1.49 us  [shards(): log_sum.reshape(nb, BLOCK, heads).transpose(0, 2, 1)]
    psum x1 -> x0, waiting for transfers between devices: 8.74 us -> none  [shards(): totals = lax.psum(totals, 'tp')]
    all_to_all x3 -> x0, waiting for transfers between devices: 8.04 us -> none  [the longest x1 4.96 us: shards(): lax.all_to_all(sent_back, 'kv', split_axis=0, concat_axis=0, tiled=True)]
    gather x3 -> x0, local copies, waits for them, and re-layouts: 6.76 us -> none  [the longest x2 6.17 us: shards(): gathered = jnp.take(block_table, slot_index.reshape(-1), axis=0)]
  transfers between devices with their start and end apart: 5 -> 0, of which waited for: 5 -> 0; matrix products, arithmetic and copies ran while one was open for 11% -> 0% of each run, Pallas kernels for 0% -> 0%
where the time goes in v1:
time: 112 us; the launch traced here: 110 us
  Pallas kernels  95.8 us (86%)
  local copies, waits for them, and re-layouts  10.7 us (10%)
  other arithmetic  2.81 us (3%)
    pallas_call x1, Pallas kernels, shards(): pl.pallas_call(functools.partial(reduce_kernel, n, tp, nb), out_shape=(ja...  66 us
    pallas_call x1, Pallas kernels, shards(): pl.pallas_call(functools.partial(fetch_kernel, n, nb), out_shape=(jax.Sha...  15.3 us
    pallas_call x1, Pallas kernels, shards(): pl.pallas_call(functools.partial(attention_kernel, heads, nb, n), out_sha...  14.5 us
    unnamed x5, local copies, waits for them, and re-layouts  8.51 us

profile of v1, /device:TPU:0, one launch (start us, length us, event | category | flops | bytes accessed | tf_op | source)
XLA Modules:
  0.0 110.0 jit_solution(16081664908434869868)
XLA Ops:
  0.6 0.7 compare_and_fusion
  1.3 2.0 %multiply_select_fusion = (s32[8,16]{1,0:T(8,128)}, s32[8,16]{1,0:T(8,128)}, s32[8,16]{1,0:T(8,128)S(1)}, s32[8]{0:T(128)}) fusion(pred[8,16]{1,0:T(8,128)(4,1)S(1)} %get-tuple-element.30, s32[8,16]{1,0:T(8,128)} %param.15, s32[8]{0:T(128)S(1)} %iota_add_fusion, s32[8,16]{1,0:T(8,128)S(1)} %get-tuple-element.29, s32[]{:T(128)S(6)} %axis_index.15), kind=kLoop, calls=%fused_computation.10 | loop fusion | flops 2552 | bytes 2756 | tf_op jit(solution)/shard_map/jit(_where)/select_n | solution.py:380
  3.3 0.1 select_reduce_fusion
  3.5 0.8 reshape.22
  4.3 0.7 reshape.23.l_ref
  4.9 0.7 broadcast_in_dim.31.want_ref
  5.7 1.6 %copy.18.keys_ref = bf16[512,64]{1,0:T(8,128)(2,1)} copy(bf16[512,64]{0,1:T(8,128)(2,1)} %param.10) | data formatting | bytes 131072 | tf_op args[2]
  7.3 1.6 %copy.19.values_ref = bf16[512,64]{1,0:T(8,128)(2,1)} copy(bf16[512,64]{0,1:T(8,128)(2,1)} %param.11) | data formatting | bytes 131072 | tf_op args[3]
  8.9 15.3 %fetch.1 = (bf16[24,64,128]{2,1,0:T(8,128)(2,1)}, s32[16,8,128]{2,1,0:T(8,128)}) custom-call(bf16[512,64]{1,0:T(8,128)(2,1)} %copy.18.keys_ref, bf16[512,64]{1,0:T(8,128)(2,1)} %copy.19.values_ref, s32[16,8,128]{2,1,0:T(8,128)} %broadcast_in_dim.31.want_ref), custom_call_target="tpu_custom_call" | custom-call | tf_op jit(solution)/shard_map/fetch/pallas_call | solution.py:383
  24.2 14.5 %attention.1 = (bf16[512,512]{1,0:T(8,128)(2,1)}, f32[8,64,128]{2,1,0:T(8,128)}, bf16[16,64,128]{2,1,0:T(8,128)(2,1)}) custom-call(s32[8,16]{1,0:T(8,128)} %get-tuple-element.32.slots, s32[8,16]{1,0:T(8,128)} %get-tuple-element.31.limits, s32[8]{0:T(128)} %get-tuple-element.34.counts, bf16[512,512]{1,0:T(8,128)(2,1)} %q_ref.1, bf16[512,512]{1,0:T(8,128)(2,1)} %o_ref.1, ...), custom_call_target="tpu_custom_call" | custom-call | tf_op jit(solution)/shard_map/attention/pallas_call | solution.py:398
  38.7 66.0 %reduce.1 = (f32[256,512]{1,0:T(8,128)}, f32[512,64]{1,0:T(8,128)}, f32[512,64]{1,0:T(8,128)}) custom-call(bf16[512,4096]{1,0:T(8,128)(2,1)} %normed_ref.1, bf16[512,512]{1,0:T(8,128)(2,1)} %get-tuple-element.39.gq_ref, f32[8,64,128]{2,1,0:T(8,128)} %get-tuple-element.14.own_ref, bf16[16,64,128]{2,1,0:T(8,128)(2,1)} %get-tuple-element.15.back_ref, ...), custom_call_target="tpu_custom_call" | custom-call | tf_op jit(solution)/shard_map/reduce/pallas_call | solution.py:434
  104.7 1.7 %copy.20 = f32[512,64]{0,1:T(8,128)} copy(f32[512,64]{1,0:T(8,128)} %get-tuple-element.25) | data formatting | bytes 262144
  106.4 1.7 %copy.21 = f32[512,64]{0,1:T(8,128)} copy(f32[512,64]{1,0:T(8,128)} %get-tuple-element.26) | data formatting | bytes 262144
  108.2 1.9 %copy.25 = f32[256,512]{1,0:T(8,128)} copy(f32[256,512]{1,0:T(8,128)} %get-tuple-element.42) | data formatting | bytes 1048576
  (2 shorter events, 0.0 us)

commit v2 on v1

--- a/solution.py
+++ b/solution.py
@@ -9,6 +9,7 @@
 
 BLOCK = 64
 GROUP = 4
+ROUNDS = 2
 NT = (((1,), (1,)), ((), ()))
 TN = (((0,), (0,)), ((), ()))
 
@@ -34,7 +35,7 @@
 def fetch_kernel(n, nb, keys_ref, values_ref, want_ref, table_ref, asked_ref, out_buf, s1, r1, s2, r2):
     me = lax.axis_index("kv")
     barrier = greet(n, 1)
-    pairs = jnp.concatenate([keys_ref[...], values_ref[...]], axis=1)
+    pairs = jnp.concatenate([keys_ref[...], values_ref[...]], axis=0).T
     for b in range(nb):
         table_ref[b] = pairs[b * BLOCK : (b + 1) * BLOCK]
 
@@ -182,7 +183,7 @@
 
 
 def reduce_kernel(
-    n, tp, nb, normed_ref, gq_ref, own_ref, back_ref, asked_ref,
+    n, tp, nb, rounds, normed_ref, gq_ref, own_ref, back_ref, asked_ref,
     wg_ref, dk_ref, dv_ref,
     gqt, send1, recv1, own, send2, recv2, send3, recv3, came, total, others,
     ss1, rs1, ss2, rs2, ss3, rs3, ssb, rsb, sst, rst,
@@ -194,11 +195,12 @@
     y = lax.rem(me // 2, 2)
     z = me // 4
     barrier = greet(n, tp)
-    half = gqt.shape[1]
-    width = send1.shape[3]
+    rows = gqt.shape[2]
+    width = send1.shape[4]
     turned = gq_ref[...].T
-    gqt[0] = turned[:half]
-    gqt[1] = turned[half:]
+    for r in range(rounds):
+        for h in range(2):
+            gqt[h, r] = turned[(2 * r + h) * rows : (2 * r + h + 1) * rows]
 
     def index(zz, a, b, h):
         return zz * 4 + (b * 2 + a if h == 0 else a * 2 + b)
@@ -211,31 +213,31 @@
         zz = lax.rem(z + 1 + lax.rem(i, zs), zs)
         return index(zz, a, bb, h)
 
-    def part(h, chunk):
+    def part(h, r, chunk):
         cols = pl.ds(pl.multiple_of(chunk * width, 128), width)
-        return jnp.dot(gqt[h], normed_ref[:, cols], preferred_element_type=jnp.float32)
-
-    def copy1(h, i):
+        return jnp.dot(gqt[h, r], normed_ref[:, cols], preferred_element_type=jnp.float32)
+
+    def copy1(h, r, i):
         a, b = coords[h]
         return pltpu.make_async_remote_copy(
-            src_ref=send1.at[h, i], dst_ref=recv1.at[h, i],
-            send_sem=ss1.at[h, i], recv_sem=rs1.at[h, i],
+            src_ref=send1.at[h, r, i], dst_ref=recv1.at[h, r, i],
+            send_sem=ss1.at[h, r, i], recv_sem=rs1.at[h, r, i],
             device_id={"kv": index(z, 1 - a, b, h)},
         )
 
-    def copy2(h, i):
+    def copy2(h, r, i):
         a, b = coords[h]
         return pltpu.make_async_remote_copy(
-            src_ref=send2.at[h, i], dst_ref=recv2.at[h, i],
-            send_sem=ss2.at[h, i], recv_sem=rs2.at[h, i],
+            src_ref=send2.at[h, r, i], dst_ref=recv2.at[h, r, i],
+            send_sem=ss2.at[h, r, i], recv_sem=rs2.at[h, r, i],
             device_id={"kv": index(z, a, 1 - b, h)},
         )
 
-    def copy3(h, i):
+    def copy3(h, r, i):
         a, b = coords[h]
         return pltpu.make_async_remote_copy(
-            src_ref=send3.at[h, i], dst_ref=recv3.at[h, i],
-            send_sem=ss3.at[h, i], recv_sem=rs3.at[h, i],
+            src_ref=send3.at[h, r, i], dst_ref=recv3.at[h, r, i],
+            send_sem=ss3.at[h, r, i], recv_sem=rs3.at[h, r, i],
             device_id={"kv": index(lax.rem(z + 1 + i, zs), a, b, h)},
         )
 
@@ -265,38 +267,42 @@
 
         lax.fori_loop(start, stop, body, 0)
 
-    def prepare(i):
-        for h in range(2):
-            send1[h, i] = part(h, chunk_at(h, i, 1 - coords[h][0])).astype(send1.dtype)
-
-    prepare(0)
-    pl.semaphore_wait(barrier, n - 1 + tp - 1)
-    for h in range(2):
-        copy1(h, 0).start()
-
-    def first(i):
-        prepare(i)
-        for h in range(2):
-            copy1(h, i).start()
-
-    loop(1, 2 * zs, first)
-    loop(0, me, lambda p: back_to(p).start())
-
-    def keep(i):
-        for h in range(2):
-            own[h, i] = part(h, chunk_at(h, i, coords[h][0]))
-
-    loop(0, 2 * zs, keep)
-
-    def second(i):
-        for h in range(2):
-            copy1(h, i).wait_recv()
-            send2[h, i] = (own[h, i] + recv1[h, i].astype(jnp.float32)).astype(send2.dtype)
-            copy2(h, i).start()
-
-    loop(0, zs, second)
-
-    total[...] = own_ref[...]
+    def prepare(r, i):
+        for h in range(2):
+            send1[h, r, i] = part(h, r, chunk_at(h, i, 1 - coords[h][0])).astype(send1.dtype)
+
+    def first(r, i):
+        prepare(r, i)
+        for h in range(2):
+            copy1(h, r, i).start()
+
+    def second(r, i):
+        for h in range(2):
+            mine_here = part(h, r, chunk_at(h, i, coords[h][0]))
+            copy1(h, r, i).wait_recv()
+            send2[h, r, i] = (mine_here + recv1[h, r, i].astype(jnp.float32)).astype(send2.dtype)
+            copy2(h, r, i).start()
+        first(r, zs + i)
+        for h in range(2):
+            own[h, r, i] = part(h, r, chunk_at(h, zs + i, coords[h][0]))
+
+    def joined(h, r, i):
+        copy1(h, r, zs + i).wait_recv()
+        copy2(h, r, i).wait_recv()
+        return (
+            own[h, r, i]
+            + recv1[h, r, zs + i].astype(jnp.float32)
+            + recv2[h, r, i].astype(jnp.float32)
+        )
+
+    def third(r, i):
+        for h in range(2):
+            send3[h, r, i] = joined(h, r, i).astype(send3.dtype)
+            copy3(h, r, i).start()
+
+    def last(r):
+        for h in range(2):
+            own[h, r, zs - 1] = joined(h, r, zs - 1)
 
     def gather(q):
         back_from(q).wait_recv()
@@ -306,51 +312,61 @@
         for b in range(nb):
             total[b] += jnp.where(wide == b, block, 0.0)
 
+    prepare(0, 0)
+    pl.semaphore_wait(barrier, n - 1 + tp - 1)
+    for h in range(2):
+        copy1(h, 0, 0).start()
+    loop(1, zs, lambda i: first(0, i))
+    loop(0, zs, lambda i: second(0, i))
+    for r in range(1, rounds):
+        loop(0, zs, lambda i: first(r, i))
+        if r == 1:
+            loop(0, me, lambda p: back_to(p).start())
+
+        def both(i):
+            third(r - 1, i)
+            second(r, i)
+
+        loop(0, zs - 1, both)
+        last(r - 1)
+        second(r, zs - 1)
+
+    total[...] = own_ref[...]
     loop(me + 1, n, gather)
     for k in range(1, tp):
         across(k).start()
-
-    def joined(h, i):
-        copy1(h, zs + i).wait_recv()
-        copy2(h, i).wait_recv()
-        return (
-            own[h, zs + i]
-            + recv1[h, zs + i].astype(jnp.float32)
-            + recv2[h, i].astype(jnp.float32)
-        )
-
-    def third(i):
-        for h in range(2):
-            send3[h, i] = joined(h, i).astype(send3.dtype)
-            copy3(h, i).start()
-
-    loop(0, zs - 1, third)
-
+    loop(0, zs - 1, lambda i: third(rounds - 1, i))
     for k in range(1, tp):
         across(k).wait_recv()
     summed = total[...]
     for k in range(1, tp):
         summed = summed + others[k - 1]
-    flat = summed.reshape(nb * BLOCK, 2 * BLOCK)
-    dk_ref[...] = flat[:, :BLOCK]
-    dv_ref[...] = flat[:, BLOCK:]
-
-    for h in range(2):
-        own[h, 0] = joined(h, zs - 1)
-
-    def fourth(i):
-        for h in range(2):
-            copy3(h, i).wait_recv()
-            own[h, 0] += recv3[h, i].astype(jnp.float32)
-
-    loop(0, zs - 1, fourth)
-    whole = jnp.concatenate([own[0, 0], own[1, 0]], axis=0)
+    flat = summed.reshape(nb * BLOCK, 2 * BLOCK).T
+    dk_ref[...] = flat[:BLOCK]
+    dv_ref[...] = flat[BLOCK:]
+
+    def finish(r):
+        def arrived(i):
+            for h in range(2):
+                copy3(h, r, i).wait_recv()
+                own[h, r, zs - 1] += recv3[h, r, i].astype(jnp.float32)
+
+        loop(0, zs - 1, arrived)
+
+    for r in range(rounds - 1):
+        finish(r)
+    last(rounds - 1)
+    finish(rounds - 1)
+    whole = jnp.concatenate(
+        [own[h, r, zs - 1] for r in range(rounds) for h in range(2)], axis=0
+    )
     wg_ref[...] = whole.T
 
-    for h in range(2):
-        loop(0, 2 * zs, lambda i: copy1(h, i).wait_send())
-        loop(0, zs, lambda i: copy2(h, i).wait_send())
-        loop(0, zs - 1, lambda i: copy3(h, i).wait_send())
+    for r in range(rounds):
+        for h in range(2):
+            loop(0, 2 * zs, lambda i: copy1(h, r, i).wait_send())
+            loop(0, zs, lambda i: copy2(h, r, i).wait_send())
+            loop(0, zs - 1, lambda i: copy3(h, r, i).wait_send())
     loop(0, me, lambda p: back_to(p).wait_send())
     for k in range(1, tp):
         across(k).wait_send()
@@ -391,7 +407,7 @@
         scratch_shapes=[pltpu.VMEM((n, BLOCK, pair), jnp.bfloat16)] + [dma((n,))] * 4,
         compiler_params=pltpu.CompilerParams(collective_id=0, has_side_effects=True),
         name="fetch",
-    )(keys, values, wanted)
+    )(keys.T, values.T, wanted)
 
     logs = log_sum.reshape(nb, BLOCK, heads).transpose(0, 2, 1).reshape(nb, 1, heads * BLOCK)
     rows_spec = pl.BlockSpec((BLOCK, cols), lambda g, *_: (g, 0))
@@ -427,34 +443,35 @@
     )(slots, limits, counts, queries, attended, cotangent, logs, table)
 
     zs = n // 4
-    half = cols // 2
+    rounds = ROUNDS
+    half = cols // (2 * rounds)
     width = model_width // n
     low = jnp.bfloat16
     wide = jnp.float32
     weight_grad, grad_keys, grad_values = pl.pallas_call(
-        functools.partial(reduce_kernel, n, tp, nb),
+        functools.partial(reduce_kernel, n, tp, nb, rounds),
         out_shape=(
             jax.ShapeDtypeStruct((width, cols), wide),
-            jax.ShapeDtypeStruct((tok_rows, BLOCK), wide),
-            jax.ShapeDtypeStruct((tok_rows, BLOCK), wide),
+            jax.ShapeDtypeStruct((BLOCK, tok_rows), wide),
+            jax.ShapeDtypeStruct((BLOCK, tok_rows), wide),
         ),
         in_specs=[vmem] * 5,
         out_specs=(vmem, vmem, vmem),
         scratch_shapes=[
-            pltpu.VMEM((2, half, tok_rows), low),
-            pltpu.VMEM((2, 2 * zs, half, width), low),
-            pltpu.VMEM((2, 2 * zs, half, width), low),
-            pltpu.VMEM((2, 2 * zs, half, width), wide),
-            pltpu.VMEM((2, zs, half, width), low),
-            pltpu.VMEM((2, zs, half, width), low),
-            pltpu.VMEM((2, zs - 1, half, width), low),
-            pltpu.VMEM((2, zs - 1, half, width), low),
+            pltpu.VMEM((2, rounds, half, tok_rows), low),
+            pltpu.VMEM((2, rounds, 2 * zs, half, width), low),
+            pltpu.VMEM((2, rounds, 2 * zs, half, width), low),
+            pltpu.VMEM((2, rounds, zs, half, width), wide),
+            pltpu.VMEM((2, rounds, zs, half, width), low),
+            pltpu.VMEM((2, rounds, zs, half, width), low),
+            pltpu.VMEM((2, rounds, zs - 1, half, width), low),
+            pltpu.VMEM((2, rounds, zs - 1, half, width), low),
             pltpu.VMEM((n, BLOCK, pair), low),
             pltpu.VMEM((nb, BLOCK, pair), wide),
             pltpu.VMEM((tp - 1, nb, BLOCK, pair), wide),
-            dma((2, 2 * zs)), dma((2, 2 * zs)),
-            dma((2, zs)), dma((2, zs)),
-            dma((2, zs - 1)), dma((2, zs - 1)),
+            dma((2, rounds, 2 * zs)), dma((2, rounds, 2 * zs)),
+            dma((2, rounds, zs)), dma((2, rounds, zs)),
+            dma((2, rounds, zs - 1)), dma((2, rounds, zs - 1)),
             dma((n,)), dma((n,)),
             dma((tp - 1,)), dma((tp - 1,)),
         ],
@@ -463,7 +480,7 @@
         ),
         name="reduce",
     )(normed, gq, own_part, back, asked)
-    return (gq, grad_keys, grad_values, weight_grad)
+    return (gq, grad_keys.T, grad_values.T, weight_grad)
 
 
 def solution(mesh):

time: 112 us -> 101 us (0.902); the launches traced: 110 us -> 101 us
  Pallas kernels: 95.8 us -> 89.8 us
  local copies, waits for them, and re-layouts: 10.7 us -> 7.21 us
    pallas_call x1, Pallas kernels: 66 us -> 60.1 us  [shards(): pl.pallas_call(functools.partial(reduce_kernel, n, tp, nb, rounds), out_s...]
    unnamed x5 -> x3, local copies, waits for them, and re-layouts: 8.51 us -> 5 us
where the time goes in v2:
time: 101 us
  Pallas kernels  89.8 us (89%)
  local copies, waits for them, and re-layouts  7.21 us (7%)
  other arithmetic  2.89 us (3%)
    pallas_call x1, Pallas kernels, shards(): pl.pallas_call(functools.partial(reduce_kernel, n, tp, nb, rounds), out_s...  60.1 us
    pallas_call x1, Pallas kernels, shards(): pl.pallas_call(functools.partial(fetch_kernel, n, nb), out_shape=(jax.Sha...  15.3 us
    pallas_call x1, Pallas kernels, shards(): pl.pallas_call(functools.partial(attention_kernel, heads, nb, n), out_sha...  14.5 us
    unnamed x3, local copies, waits for them, and re-layouts  5 us
    select_n x1, other arithmetic, shards(): limits = jnp.where(listed, (chosen - row_base) * BLOCK, 4 * BLOCK)  2.05 us

profile of v2, /device:TPU:0, one launch (start us, length us, event | category | flops | bytes accessed | tf_op | source)
XLA Modules:
  0.0 100.6 jit_solution(6237500976639830427)
XLA Ops:
  0.6 0.7 compare_and_fusion
  1.3 2.0 %multiply_select_fusion = (s32[8,16]{1,0:T(8,128)}, s32[8,16]{1,0:T(8,128)}, s32[8,16]{1,0:T(8,128)S(1)}, s32[8]{0:T(128)}) fusion(pred[8,16]{1,0:T(8,128)(4,1)S(1)} %get-tuple-element.22, s32[8,16]{1,0:T(8,128)} %param.15, s32[8]{0:T(128)S(1)} %iota_add_fusion, s32[8,16]{1,0:T(8,128)S(1)} %get-tuple-element.21, s32[]{:T(128)S(6)} %axis_index.15), kind=kLoop, calls=%fused_computation.10 | loop fusion | flops 2552 | bytes 2756 | tf_op jit(solution)/shard_map/jit(_where)/select_n | solution.py:396
  3.4 0.1 select_reduce_fusion
  3.5 0.8 reshape.22
  4.3 0.7 reshape.23.l_ref
  5.0 0.7 broadcast_in_dim.31.want_ref
  5.7 15.3 %fetch.1 = (bf16[24,64,128]{2,1,0:T(8,128)(2,1)}, s32[16,8,128]{2,1,0:T(8,128)}) custom-call(bf16[64,512]{1,0:T(8,128)(2,1)} %bitcast.12, bf16[64,512]{1,0:T(8,128)(2,1)} %bitcast.13, s32[16,8,128]{2,1,0:T(8,128)} %broadcast_in_dim.31.want_ref), custom_call_target="tpu_custom_call" | custom-call | tf_op jit(solution)/shard_map/fetch/pallas_call | solution.py:399
  21.0 14.5 %attention.1 = (bf16[512,512]{1,0:T(8,128)(2,1)}, f32[8,64,128]{2,1,0:T(8,128)}, bf16[16,64,128]{2,1,0:T(8,128)(2,1)}) custom-call(s32[8,16]{1,0:T(8,128)} %get-tuple-element.24.slots, s32[8,16]{1,0:T(8,128)} %get-tuple-element.23.limits, s32[8]{0:T(128)} %get-tuple-element.26.counts, bf16[512,512]{1,0:T(8,128)(2,1)} %q_ref.1, bf16[512,512]{1,0:T(8,128)(2,1)} %o_ref.1, ...), custom_call_target="tpu_custom_call" | custom-call | tf_op jit(solution)/shard_map/attention/pallas_call | solution.py:414
  35.5 60.1 %reduce.1 = (f32[256,512]{1,0:T(8,128)}, f32[64,512]{1,0:T(8,128)}, f32[64,512]{1,0:T(8,128)}) custom-call(bf16[512,4096]{1,0:T(8,128)(2,1)} %normed_ref.1, bf16[512,512]{1,0:T(8,128)(2,1)} %get-tuple-element.31.gq_ref, f32[8,64,128]{2,1,0:T(8,128)} %get-tuple-element.14.own_ref, bf16[16,64,128]{2,1,0:T(8,128)(2,1)} %get-tuple-element.15.back_ref, ...), custom_call_target="tpu_custom_call" | custom-call | tf_op jit(solution)/shard_map/reduce/pallas_call | solution.py:451
  95.6 1.6 %copy.19 = f32[512,64]{0,1:T(8,128)} copy(f32[512,64]{0,1:T(8,128)} %bitcast.10) | data formatting | bytes 262144
  97.2 1.6 %copy.20 = f32[512,64]{0,1:T(8,128)} copy(f32[512,64]{0,1:T(8,128)} %bitcast.9) | data formatting | bytes 262144
  98.7 1.9 %copy.21 = f32[256,512]{1,0:T(8,128)} copy(f32[256,512]{1,0:T(8,128)} %get-tuple-element.34) | data formatting | bytes 1048576
  (2 shorter events, 0.0 us)

commit v3 on v2

--- a/solution.py
+++ b/solution.py
@@ -32,7 +32,9 @@
     return barrier
 
 
-def fetch_kernel(n, nb, keys_ref, values_ref, want_ref, table_ref, asked_ref, out_buf, s1, r1, s2, r2):
+def fetch_kernel(
+    n, nb, keys_ref, values_ref, chosen_ref, table_ref, asked_ref, want_ref, out_buf, s1, r1, s2, r2
+):
     me = lax.axis_index("kv")
     barrier = greet(n, 1)
     pairs = jnp.concatenate([keys_ref[...], values_ref[...]], axis=0).T
@@ -50,6 +52,16 @@
         return 0
 
     lax.fori_loop(0, me + 1, unasked, 0)
+    ids = chosen_ref[...]
+
+    def want(p, _):
+        inner = ids - p * nb
+        best = jnp.where((inner >= 0) & (inner < nb), inner, -1)
+        best = jnp.max(jnp.max(best, axis=1, keepdims=True), axis=0, keepdims=True)
+        want_ref[p] = jnp.broadcast_to(best, want_ref.shape[1:])
+        return 0
+
+    lax.fori_loop(0, me, want, 0)
     pl.semaphore_wait(barrier, n - 1)
 
     def request(p):
@@ -114,16 +126,29 @@
 
 
 def attention_kernel(
-    heads, nb, n, slots, limits, counts,
-    q_ref, o_ref, g_ref, l_ref, table_ref, gq_ref, own_ref, back_ref, acc, dqt,
+    heads, nb, n, chosen,
+    q_ref, o_ref, g_ref, l_ref, table_ref, gq_ref, own_ref, back_ref, acc, dqt, lines,
 ):
     g = pl.program_id(0)
+    me = lax.axis_index("kv")
     rows = heads * BLOCK
     scale = BLOCK ** (-0.5)
 
     @pl.when(g == 0)
     def _():
         acc[...] = jnp.zeros_like(acc)
+        for b in range(nb):
+            lines[b] = jnp.concatenate(
+                [l_ref[h : h + 1, b * BLOCK : (b + 1) * BLOCK] for h in range(heads)], axis=1
+            )
+
+    def slot_of(c):
+        inner = c - me * nb
+        near = (inner >= 0) & (inner < nb)
+        return jnp.where(c < 0, 0, jnp.where(near, inner, nb + c // nb))
+
+    def limit_of(c):
+        return jnp.where(c < 0, 4 * BLOCK, (c - (me * nb + g)) * BLOCK)
 
     def stack(ref):
         full = ref[...]
@@ -139,17 +164,18 @@
         lax.dot_general(ones, high, NT, preferred_element_type=jnp.float32)
         + lax.dot_general(ones, low, NT, preferred_element_type=jnp.float32)
     )[0:1]
-    logs = l_ref[0]
+    logs = lines[g]
     ahead = (
         lax.broadcasted_iota(jnp.int32, (BLOCK, rows), 1) % BLOCK
         - lax.broadcasted_iota(jnp.int32, (BLOCK, rows), 0)
     )
     dqt[...] = jnp.zeros_like(dqt)
-    for c in range(slots.shape[1] // GROUP):
-
-        @pl.when(counts[g] > c * GROUP)
+    for c in range(chosen.shape[1] // GROUP):
+
+        @pl.when(chosen[g, c * GROUP] >= 0)
         def _():
-            ids = [slots[g, c * GROUP + i] for i in range(GROUP)]
+            listed = [chosen[g, c * GROUP + i] for i in range(GROUP)]
+            ids = [slot_of(v) for v in listed]
             pairs = jnp.concatenate([table_ref[s] for s in ids], axis=0)
             k = pairs[:, :BLOCK]
             v = pairs[:, BLOCK:]
@@ -159,7 +185,7 @@
             p = jnp.concatenate(
                 [
                     jnp.where(
-                        ahead >= limits[g, c * GROUP + i], e[i * BLOCK : (i + 1) * BLOCK], 0.0
+                        ahead >= limit_of(listed[i]), e[i * BLOCK : (i + 1) * BLOCK], 0.0
                     )
                     for i in range(GROUP)
                 ],
@@ -184,7 +210,7 @@
 
 def reduce_kernel(
     n, tp, nb, rounds, normed_ref, gq_ref, own_ref, back_ref, asked_ref,
-    wg_ref, dk_ref, dv_ref,
+    wgt_ref, dkv_ref,
     gqt, send1, recv1, own, send2, recv2, send3, recv3, came, total, others,
     ss1, rs1, ss2, rs2, ss3, rs3, ssb, rsb, sst, rst,
 ):
@@ -341,9 +367,7 @@
     summed = total[...]
     for k in range(1, tp):
         summed = summed + others[k - 1]
-    flat = summed.reshape(nb * BLOCK, 2 * BLOCK).T
-    dk_ref[...] = flat[:BLOCK]
-    dv_ref[...] = flat[BLOCK:]
+    dkv_ref[...] = summed.reshape(nb * BLOCK, 2 * BLOCK)
 
     def finish(r):
         def arrived(i):
@@ -357,10 +381,9 @@
         finish(r)
     last(rounds - 1)
     finish(rounds - 1)
-    whole = jnp.concatenate(
-        [own[h, r, zs - 1] for r in range(rounds) for h in range(2)], axis=0
-    )
-    wg_ref[...] = whole.T
+    for r in range(rounds):
+        for h in range(2):
+            wgt_ref[(2 * r + h) * rows : (2 * r + h + 1) * rows] = own[h, r, zs - 1]
 
     for r in range(rounds):
         for h in range(2):
@@ -372,29 +395,21 @@
         across(k).wait_send()
 
 
+def turn_kernel(wgt_ref, dkv_ref, wg_ref, dk_ref, dv_ref):
+    wg_ref[...] = wgt_ref[...].T
+    flat = dkv_ref[...].T
+    dk_ref[...] = flat[:BLOCK]
+    dv_ref[...] = flat[BLOCK:]
+
+
 def shards(n, tp, normed, queries, keys, values, attended, cotangent, log_sum, chosen):
-    me = lax.axis_index("kv")
     tok_rows, model_width = normed.shape
-    slot_count = chosen.shape[1]
     nb = tok_rows // BLOCK
     heads = log_sum.shape[1]
     cols = queries.shape[1]
     pair = 2 * BLOCK
     vmem = pl.BlockSpec(memory_space=pltpu.VMEM)
     dma = pltpu.SemaphoreType.DMA
-
-    owners = chosen // nb
-    within = chosen % nb
-    listed = chosen >= 0
-    remote = listed & (owners != me)
-    peer_ids = jnp.arange(n, dtype=jnp.int32)
-    matched = remote[:, :, None] & (owners[:, :, None] == peer_ids)
-    wanted = jnp.max(jnp.where(matched, within[:, :, None], -1), axis=(0, 1))
-    wanted = jnp.broadcast_to(wanted[:, None, None], (n, 8, 128))
-    slots = jnp.where(listed, jnp.where(owners == me, within, nb + owners), 0)
-    row_base = (me * nb + jnp.arange(nb, dtype=jnp.int32))[:, None]
-    limits = jnp.where(listed, (chosen - row_base) * BLOCK, 4 * BLOCK)
-    counts = jnp.sum(listed.astype(jnp.int32), axis=1)
 
     table, asked = pl.pallas_call(
         functools.partial(fetch_kernel, n, nb),
@@ -404,12 +419,15 @@
         ),
         in_specs=[vmem] * 3,
         out_specs=(vmem, vmem),
-        scratch_shapes=[pltpu.VMEM((n, BLOCK, pair), jnp.bfloat16)] + [dma((n,))] * 4,
+        scratch_shapes=[
+            pltpu.VMEM((n, 8, 128), jnp.int32),
+            pltpu.VMEM((n, BLOCK, pair), jnp.bfloat16),
+        ]
+        + [dma((n,))] * 4,
         compiler_params=pltpu.CompilerParams(collective_id=0, has_side_effects=True),
         name="fetch",
-    )(keys.T, values.T, wanted)
-
-    logs = log_sum.reshape(nb, BLOCK, heads).transpose(0, 2, 1).reshape(nb, 1, heads * BLOCK)
+    )(keys.T, values.T, chosen)
+
     rows_spec = pl.BlockSpec((BLOCK, cols), lambda g, *_: (g, 0))
     gq, own_part, back = pl.pallas_call(
         functools.partial(attention_kernel, heads, nb, n),
@@ -419,13 +437,13 @@
             jax.ShapeDtypeStruct((n, BLOCK, pair), jnp.bfloat16),
         ),
         grid_spec=pltpu.PrefetchScalarGridSpec(
-            num_scalar_prefetch=3,
+            num_scalar_prefetch=1,
             grid=(nb,),
             in_specs=[
                 rows_spec,
                 rows_spec,
                 rows_spec,
-                pl.BlockSpec((1, 1, heads * BLOCK), lambda g, *_: (g, 0, 0)),
+                pl.BlockSpec((heads, tok_rows), lambda g, *_: (0, 0)),
                 pl.BlockSpec((nb + n, BLOCK, pair), lambda g, *_: (0, 0, 0)),
             ],
             out_specs=(
@@ -436,11 +454,12 @@
             scratch_shapes=[
                 pltpu.VMEM((nb + n, BLOCK, pair), jnp.float32),
                 pltpu.VMEM((BLOCK, heads * BLOCK), jnp.float32),
+                pltpu.VMEM((nb, 1, heads * BLOCK), jnp.float32),
             ],
         ),
         compiler_params=pltpu.CompilerParams(dimension_semantics=("arbitrary",)),
         name="attention",
-    )(slots, limits, counts, queries, attended, cotangent, logs, table)
+    )(chosen, queries, attended, cotangent, log_sum.T, table)
 
     zs = n // 4
     rounds = ROUNDS
@@ -448,15 +467,14 @@
     width = model_width // n
     low = jnp.bfloat16
     wide = jnp.float32
-    weight_grad, grad_keys, grad_values = pl.pallas_call(
+    turned, dkv = pl.pallas_call(
         functools.partial(reduce_kernel, n, tp, nb, rounds),
         out_shape=(
-            jax.ShapeDtypeStruct((width, cols), wide),
-            jax.ShapeDtypeStruct((BLOCK, tok_rows), wide),
-            jax.ShapeDtypeStruct((BLOCK, tok_rows), wide),
+            jax.ShapeDtypeStruct((cols, width), wide),
+            jax.ShapeDtypeStruct((tok_rows, pair), wide),
         ),
         in_specs=[vmem] * 5,
-        out_specs=(vmem, vmem, vmem),
+        out_specs=(vmem, vmem),
         scratch_shapes=[
             pltpu.VMEM((2, rounds, half, tok_rows), low),
             pltpu.VMEM((2, rounds, 2 * zs, half, width), low),
@@ -480,6 +498,17 @@
         ),
         name="reduce",
     )(normed, gq, own_part, back, asked)
+    weight_grad, grad_keys, grad_values = pl.pallas_call(
+        turn_kernel,
+        out_shape=(
+            jax.ShapeDtypeStruct((width, cols), wide),
+            jax.ShapeDtypeStruct((BLOCK, tok_rows), wide),
+            jax.ShapeDtypeStruct((BLOCK, tok_rows), wide),
+        ),
+        in_specs=[vmem] * 2,
+        out_specs=(vmem, vmem, vmem),
+        name="turn",
+    )(turned, dkv)
     return (gq, grad_keys.T, grad_values.T, weight_grad)
 
 

time: 101 us -> 91.9 us (0.910)
  local copies, waits for them, and re-layouts: 7.21 us -> 0 us
  other arithmetic: 2.89 us -> 0 us
    unnamed x3 -> x0, local copies, waits for them, and re-layouts: 5 us -> none
    pallas_call x0 -> x1, Pallas kernels: none -> 2.18 us  [shards(): pl.pallas_call(turn_kernel, out_shape=(jax.ShapeDtypeStruct((width, cols)...]
    select_n x1 -> x0, other arithmetic: 2.05 us -> none  [shards(): limits = jnp.where(listed, (chosen - row_base) * BLOCK, 4 * BLOCK)]
    pallas_call x1, Pallas kernels: 60.1 us -> 58.3 us  [shards(): pl.pallas_call(functools.partial(reduce_kernel, n, tp, nb, rounds), out_s...]
    reshape x3 -> x0, local copies, waits for them, and re-layouts: 1.5 us -> none  [shards(): log_sum.reshape(nb, BLOCK, heads).transpose(0, 2, 1)]
where the time goes in v3:
time: 91.9 us; the launch traced here: 90.6 us
  Pallas kernels  90 us (98%)
    pallas_call x1, Pallas kernels, shards(): pl.pallas_call(functools.partial(reduce_kernel, n, tp, nb, rounds), out_s...  58.3 us
    pallas_call x1, Pallas kernels, shards(): pl.pallas_call(functools.partial(fetch_kernel, n, nb), out_shape=(jax.Sha...  14.9 us
    pallas_call x1, Pallas kernels, shards(): pl.pallas_call(functools.partial(attention_kernel, heads, nb, n), out_sha...  14.6 us
    pallas_call x1, Pallas kernels, shards(): pl.pallas_call(turn_kernel, out_shape=(jax.ShapeDtypeStruct((width, cols)...  2.18 us

profile of v3, /device:TPU:0, one launch (start us, length us, event | category | flops | bytes accessed | tf_op | source)
XLA Modules:
  0.0 90.6 jit_solution(10162255683968930869)
XLA Ops:
  0.6 14.9 %fetch.1 = (bf16[24,64,128]{2,1,0:T(8,128)(2,1)}, s32[16,8,128]{2,1,0:T(8,128)}) custom-call(bf16[64,512]{1,0:T(8,128)(2,1)} %bitcast.5, bf16[64,512]{1,0:T(8,128)(2,1)} %bitcast.6, s32[8,16]{1,0:T(8,128)} %chosen.1), custom_call_target="tpu_custom_call" | custom-call | tf_op jit(solution)/shard_map/fetch/pallas_call | solution.py:414
  15.5 14.6 %attention.1 = (bf16[512,512]{1,0:T(8,128)(2,1)}, f32[8,64,128]{2,1,0:T(8,128)}, bf16[16,64,128]{2,1,0:T(8,128)(2,1)}) custom-call(s32[8,16]{1,0:T(8,128)} %chosen.1, bf16[512,512]{1,0:T(8,128)(2,1)} %q_ref.1, bf16[512,512]{1,0:T(8,128)(2,1)} %o_ref.1, bf16[512,512]{1,0:T(8,128)(2,1)} %g_ref.1, f32[8,512]{1,0:T(8,128)} %bitcast.7, ...), custom_call_target="tpu_custom_call" | custom-call | tf_op jit(solution)/shard_map/attention/pallas_call | solution.py:432
  30.1 58.3 %reduce.1 = (f32[512,256]{1,0:T(8,128)}, f32[512,128]{1,0:T(8,128)}) custom-call(bf16[512,4096]{1,0:T(8,128)(2,1)} %normed_ref.1, bf16[512,512]{1,0:T(8,128)(2,1)} %get-tuple-element.10.gq_ref, f32[8,64,128]{2,1,0:T(8,128)} %get-tuple-element.16.own_ref, bf16[16,64,128]{2,1,0:T(8,128)(2,1)} %get-tuple-element.17.back_ref, ...), custom_call_target="tpu_custom_call" | custom-call | tf_op jit(solution)/shard_map/reduce/pallas_call | solution.py:470
  88.4 2.2 %turn.1 = (f32[256,512]{1,0:T(8,128)}, f32[64,512]{1,0:T(8,128)}, f32[64,512]{1,0:T(8,128)}) custom-call(f32[512,256]{1,0:T(8,128)} %get-tuple-element.19.wgt_ref, f32[512,128]{1,0:T(8,128)} %get-tuple-element.20.dkv_ref), custom_call_target="tpu_custom_call" | custom-call | tf_op jit(solution)/shard_map/turn/pallas_call | solution.py:501

commit v4 on v3

--- a/solution.py
+++ b/solution.py
@@ -8,7 +8,7 @@
 from jax.sharding import PartitionSpec as P
 
 BLOCK = 64
-GROUP = 4
+GROUP = 16
 ROUNDS = 2
 NT = (((1,), (1,)), ((), ()))
 TN = (((0,), (0,)), ((), ()))

time: 91.9 us -> 86.9 us (0.946); the launches traced: 90.6 us -> 86.7 us
  Pallas kernels: 90 us -> 86 us
    pallas_call x1, Pallas kernels: 58.3 us -> 50.7 us  [shards(): pl.pallas_call(functools.partial(reduce_kernel, n, tp, nb, rounds), out_s...]
    pallas_call x1, Pallas kernels: 14.6 us -> 18.2 us  [shards(): pl.pallas_call(functools.partial(attention_kernel, heads, nb, n), out_sha...]
where the time goes in v4:
time: 86.9 us; the launch traced here: 86.7 us
  Pallas kernels  86 us (99%)
    pallas_call x1, Pallas kernels, shards(): pl.pallas_call(functools.partial(reduce_kernel, n, tp, nb, rounds), out_s...  50.7 us
    pallas_call x1, Pallas kernels, shards(): pl.pallas_call(functools.partial(attention_kernel, heads, nb, n), out_sha...  18.2 us
    pallas_call x1, Pallas kernels, shards(): pl.pallas_call(functools.partial(fetch_kernel, n, nb), out_shape=(jax.Sha...  14.9 us
    pallas_call x1, Pallas kernels, shards(): pl.pallas_call(turn_kernel, out_shape=(jax.ShapeDtypeStruct((width, cols)...  2.18 us

profile of v4, /device:TPU:0, one launch (start us, length us, event | category | flops | bytes accessed | tf_op | source)
XLA Modules:
  0.0 86.7 jit_solution(17350804447525319364)
XLA Ops:
  0.6 14.9 %fetch.1 = (bf16[24,64,128]{2,1,0:T(8,128)(2,1)}, s32[16,8,128]{2,1,0:T(8,128)}) custom-call(bf16[64,512]{1,0:T(8,128)(2,1)} %bitcast.5, bf16[64,512]{1,0:T(8,128)(2,1)} %bitcast.6, s32[8,16]{1,0:T(8,128)} %chosen.1), custom_call_target="tpu_custom_call" | custom-call | tf_op jit(solution)/shard_map/fetch/pallas_call | solution.py:414
  15.5 18.2 %attention.1 = (bf16[512,512]{1,0:T(8,128)(2,1)}, f32[8,64,128]{2,1,0:T(8,128)}, bf16[16,64,128]{2,1,0:T(8,128)(2,1)}) custom-call(s32[8,16]{1,0:T(8,128)} %chosen.1, bf16[512,512]{1,0:T(8,128)(2,1)} %q_ref.1, bf16[512,512]{1,0:T(8,128)(2,1)} %o_ref.1, bf16[512,512]{1,0:T(8,128)(2,1)} %g_ref.1, f32[8,512]{1,0:T(8,128)} %bitcast.7, ...), custom_call_target="tpu_custom_call" | custom-call | tf_op jit(solution)/shard_map/attention/pallas_call | solution.py:432
  33.8 50.7 %reduce.1 = (f32[512,256]{1,0:T(8,128)}, f32[512,128]{1,0:T(8,128)}) custom-call(bf16[512,4096]{1,0:T(8,128)(2,1)} %normed_ref.1, bf16[512,512]{1,0:T(8,128)(2,1)} %get-tuple-element.10.gq_ref, f32[8,64,128]{2,1,0:T(8,128)} %get-tuple-element.16.own_ref, bf16[16,64,128]{2,1,0:T(8,128)(2,1)} %get-tuple-element.17.back_ref, ...), custom_call_target="tpu_custom_call" | custom-call | tf_op jit(solution)/shard_map/reduce/pallas_call | solution.py:470
  84.5 2.2 %turn.1 = (f32[256,512]{1,0:T(8,128)}, f32[64,512]{1,0:T(8,128)}, f32[64,512]{1,0:T(8,128)}) custom-call(f32[512,256]{1,0:T(8,128)} %get-tuple-element.19.wgt_ref, f32[512,128]{1,0:T(8,128)} %get-tuple-element.20.dkv_ref), custom_call_target="tpu_custom_call" | custom-call | tf_op jit(solution)/shard_map/turn/pallas_call | solution.py:501

commit v5 on v4

--- a/solution.py
+++ b/solution.py
@@ -154,7 +154,7 @@
         full = ref[...]
         return jnp.concatenate([full[:, h * BLOCK : (h + 1) * BLOCK] for h in range(heads)], axis=0)
 
-    q = stack(q_ref)
+    q = stack(q_ref) * jnp.bfloat16(scale)
     go = stack(g_ref)
     prod = go.astype(jnp.float32) * stack(o_ref).astype(jnp.float32)
     high = prod.astype(jnp.bfloat16)
@@ -181,7 +181,7 @@
             v = pairs[:, BLOCK:]
             s = lax.dot_general(k, q, NT, preferred_element_type=jnp.float32)
             dp = lax.dot_general(v, go, NT, preferred_element_type=jnp.float32)
-            e = jnp.exp(s * scale - logs)
+            e = jnp.exp(s - logs)
             p = jnp.concatenate(
                 [
                     jnp.where(
@@ -191,7 +191,7 @@
                 ],
                 axis=0,
             )
-            ds = (p * (dp - delta) * scale).astype(jnp.bfloat16)
+            ds = (p * (dp - delta)).astype(jnp.bfloat16)
             dk = jnp.dot(ds, q, preferred_element_type=jnp.float32)
             dv = jnp.dot(p.astype(jnp.bfloat16), go, preferred_element_type=jnp.float32)
             dqt[...] += lax.dot_general(k, ds, TN, preferred_element_type=jnp.float32)
@@ -199,7 +199,7 @@
             for i in range(GROUP):
                 acc[ids[i]] += dkv[i * BLOCK : (i + 1) * BLOCK]
 
-    dq = dqt[...].T.astype(jnp.bfloat16)
+    dq = (dqt[...] * scale).T.astype(jnp.bfloat16)
     gq_ref[...] = jnp.concatenate([dq[h * BLOCK : (h + 1) * BLOCK] for h in range(heads)], axis=1)
 
     @pl.when(g == nb - 1)
@@ -209,10 +209,10 @@
 
 
 def reduce_kernel(
-    n, tp, nb, rounds, normed_ref, gq_ref, own_ref, back_ref, asked_ref,
+    n, tp, nb, rounds, normed_hbm, gq_ref, own_ref, back_ref, asked_ref,
     wgt_ref, dkv_ref,
     gqt, send1, recv1, own, send2, recv2, send3, recv3, came, total, others,
-    ss1, rs1, ss2, rs2, ss3, rs3, ssb, rsb, sst, rst,
+    ss1, rs1, ss2, rs2, ss3, rs3, ssb, rsb, sst, rst, normed_ref, load_sem,
 ):
     me = lax.axis_index("kv")
     mine = lax.axis_index("tp")
@@ -220,6 +220,8 @@
     x = lax.rem(me, 2)
     y = lax.rem(me // 2, 2)
     z = me // 4
+    load = pltpu.make_async_copy(normed_hbm, normed_ref, load_sem)
+    load.start()
     barrier = greet(n, tp)
     rows = gqt.shape[2]
     width = send1.shape[4]
@@ -338,6 +340,7 @@
         for b in range(nb):
             total[b] += jnp.where(wide == b, block, 0.0)
 
+    load.wait()
     prepare(0, 0)
     pl.semaphore_wait(barrier, n - 1 + tp - 1)
     for h in range(2):
@@ -473,7 +476,7 @@
             jax.ShapeDtypeStruct((cols, width), wide),
             jax.ShapeDtypeStruct((tok_rows, pair), wide),
         ),
-        in_specs=[vmem] * 5,
+        in_specs=[pl.BlockSpec(memory_space=pl.ANY)] + [vmem] * 4,
         out_specs=(vmem, vmem),
         scratch_shapes=[
             pltpu.VMEM((2, rounds, half, tok_rows), low),
@@ -492,6 +495,7 @@
             dma((2, rounds, zs - 1)), dma((2, rounds, zs - 1)),
             dma((n,)), dma((n,)),
             dma((tp - 1,)), dma((tp - 1,)),
+            pltpu.VMEM((tok_rows, model_width), low), dma,
         ],
         compiler_params=pltpu.CompilerParams(
             collective_id=1, has_side_effects=True, vmem_limit_bytes=56 * 1024 * 1024

time: 86.9 us -> 86.4 us (level)
  no operation moved by 1% of the time
where the time goes in v5:
time: 86.4 us; the launch traced here: 86.1 us
  Pallas kernels  85.4 us (99%)
    pallas_call x1, Pallas kernels, shards(): pl.pallas_call(functools.partial(reduce_kernel, n, tp, nb, rounds), out_s...  50.2 us
    pallas_call x1, Pallas kernels, shards(): pl.pallas_call(functools.partial(attention_kernel, heads, nb, n), out_sha...  18.1 us
    pallas_call x1, Pallas kernels, shards(): pl.pallas_call(functools.partial(fetch_kernel, n, nb), out_shape=(jax.Sha...  14.9 us
    pallas_call x1, Pallas kernels, shards(): pl.pallas_call(turn_kernel, out_shape=(jax.ShapeDtypeStruct((width, cols)...  2.18 us

profile of v5, /device:TPU:0, one launch (start us, length us, event | category | flops | bytes accessed | tf_op | source)
XLA Modules:
  0.0 86.1 jit_solution(8160325453600863002)
XLA Ops:
  0.6 14.9 %fetch.1 = (bf16[24,64,128]{2,1,0:T(8,128)(2,1)}, s32[16,8,128]{2,1,0:T(8,128)}) custom-call(bf16[64,512]{1,0:T(8,128)(2,1)} %bitcast.5, bf16[64,512]{1,0:T(8,128)(2,1)} %bitcast.6, s32[8,16]{1,0:T(8,128)} %chosen.1), custom_call_target="tpu_custom_call" | custom-call | tf_op jit(solution)/shard_map/fetch/pallas_call | solution.py:417
  15.5 18.1 %attention.1 = (bf16[512,512]{1,0:T(8,128)(2,1)}, f32[8,64,128]{2,1,0:T(8,128)}, bf16[16,64,128]{2,1,0:T(8,128)(2,1)}) custom-call(s32[8,16]{1,0:T(8,128)} %chosen.1, bf16[512,512]{1,0:T(8,128)(2,1)} %q_ref.1, bf16[512,512]{1,0:T(8,128)(2,1)} %o_ref.1, bf16[512,512]{1,0:T(8,128)(2,1)} %g_ref.1, f32[8,512]{1,0:T(8,128)} %bitcast.7, ...), custom_call_target="tpu_custom_call" | custom-call | tf_op jit(solution)/shard_map/attention/pallas_call | solution.py:435
  33.7 50.2 %reduce.1 = (f32[512,256]{1,0:T(8,128)}, f32[512,128]{1,0:T(8,128)}) custom-call(bf16[512,4096]{1,0:T(8,128)(2,1)} %normed_hbm.1, bf16[512,512]{1,0:T(8,128)(2,1)} %get-tuple-element.10.gq_ref, f32[8,64,128]{2,1,0:T(8,128)} %get-tuple-element.16.own_ref, bf16[16,64,128]{2,1,0:T(8,128)(2,1)} %get-tuple-element.17.back_ref, ...), custom_call_target="tpu_custom_call" | custom-call | tf_op jit(solution)/shard_map/reduce/pallas_call | solution.py:473
  83.9 2.2 %turn.1 = (f32[256,512]{1,0:T(8,128)}, f32[64,512]{1,0:T(8,128)}, f32[64,512]{1,0:T(8,128)}) custom-call(f32[512,256]{1,0:T(8,128)} %get-tuple-element.19.wgt_ref, f32[512,128]{1,0:T(8,128)} %get-tuple-element.20.dkv_ref), custom_call_target="tpu_custom_call" | custom-call | tf_op jit(solution)/shard_map/turn/pallas_call | solution.py:505
